TPU v7x, 32 devices: a whole 2x2x4 slice. The times are simulated.
32 devices in a mesh: fs: 16 (over z, y, x), tp: 2 (over core).
Axes of the slice: x: 2, y: 2, z: 4, core: 2. Of those that a mesh axis runs over, the one named last changes fastest.
Arguments:
- normed: bfloat16 [16384, 2048], P('fs'), may hold values from -6 to 6
- key_cot: bfloat16 [16384, 1024], P('fs', 'tp'), may hold values from -130 to 130
- value_cot: bfloat16 [16384, 2048], P('fs', 'tp'), may hold values from -130 to 130
- basis: bfloat16 [2048, 256], P('fs'), may hold values from -3.535534 to 3.535534
- master_key: float32 [2048, 1024], P('fs', 'tp'), may hold values from -3 to 3
- master_value: float32 [2048, 2048], P('fs', 'tp'), may hold values from -3 to 3
- first_key: float32 [256, 1024], P('fs', 'tp'), may hold values from -3 to 3
- second_key: float32 [256, 1024], P('fs', 'tp'), may hold values from 0.05 to 2
- first_value: float32 [256, 2048], P('fs', 'tp'), may hold values from -3 to 3
- second_value: float32 [256, 2048], P('fs', 'tp'), may hold values from 0.05 to 2
Outputs:
- step_key: float32 [2048, 1024], P('fs', 'tp')
- step_value: float32 [2048, 2048], P('fs', 'tp')
- new_master_key: float32 [2048, 1024], P('fs', 'tp')
- new_master_value: float32 [2048, 2048], P('fs', 'tp')
- copy_key: bfloat16 [2048, 1024], P(None, 'tp')
- copy_value: bfloat16 [2048, 2048], P(None, 'tp')
- new_first_key: float32 [256, 1024], P('fs', 'tp')
- new_second_key: float32 [256, 1024], P('fs', 'tp')
- new_first_value: float32 [256, 2048], P('fs', 'tp')
- new_second_value: float32 [256, 2048], P('fs', 'tp')
All inputs are finite; a program needn't handle non-finite values.
Results may differ from a plain program's by a relative error of at most 0.0055.
Values may be sent and summed in bfloat16 or wider, within the bound.
A program may use at most 64 MiB of HBM per device.

v0:
```python
import jax
import jax.numpy as jnp
from jax import lax
from jax.sharding import PartitionSpec as P

DK = 1024
DV = 2048
R = 256


learn_rate = 0.05
beta_first = 0.9
beta_second = 0.9
epsilon = 1e-08
norm_eps = 1e-06


def on_device(
    normed,
    key_cot,
    value_cot,
    basis,
    master_key,
    master_value,
    first_key,
    second_key,
    first_value,
    second_value,
):
    key_cols = key_cot.shape[1]
    cotangents = jnp.concatenate([key_cot, value_cot], axis=1)
    projected = jnp.dot(
        normed, lax.all_gather(basis, "fs", axis=0, tiled=True), preferred_element_type=jnp.float32
    )
    upper_part = projected.astype(jnp.bfloat16)
    lower_part = (projected - upper_part.astype(jnp.float32)).astype(jnp.bfloat16)
    partial_value = lax.dot_general(
        upper_part, cotangents, (((0,), (0,)), ((), ())), preferred_element_type=jnp.float32
    )
    partial_value = partial_value + lax.dot_general(
        lower_part, cotangents, (((0,), (0,)), ((), ())), preferred_element_type=jnp.float32
    )
    rank_rows = first_key.shape[0]
    summed = lax.psum(partial_value, "fs")
    squares = lax.psum(jnp.sum(summed * summed), "tp")
    own_rows = lax.dynamic_slice_in_dim(summed, lax.axis_index("fs") * rank_rows, rank_rows, 0)
    root_mean = jnp.sqrt(squares / (R * (DK + DV)) + norm_eps)
    grad_scale = 1.0 / root_mean
    first_moment = jnp.concatenate([first_key, first_value], axis=1)
    second_moment = jnp.concatenate([second_key, second_value], axis=1)
    scaled = own_rows * grad_scale
    new_first = beta_first * first_moment + (1.0 - beta_first) * scaled
    new_second = beta_second * second_moment + (1.0 - beta_second) * scaled * scaled
    direction = (new_first / (jnp.sqrt(new_second) + epsilon)).astype(jnp.bfloat16)
    all_directions = lax.all_gather(direction, "fs", axis=0, tiled=True)
    update_step = jnp.dot(basis, all_directions, preferred_element_type=jnp.float32)
    master = jnp.concatenate([master_key, master_value], axis=1)
    new_master = master - learn_rate * update_step
    half_copy = new_master.astype(jnp.bfloat16)
    copy_key, copy_value = (
        lax.all_gather(half_copy[:, :key_cols], "fs", axis=0, tiled=True),
        lax.all_gather(half_copy[:, key_cols:], "fs", axis=0, tiled=True),
    )
    return (
        update_step[:, :key_cols],
        update_step[:, key_cols:],
        new_master[:, :key_cols],
        new_master[:, key_cols:],
        copy_key,
        copy_value,
        new_first[:, :key_cols],
        new_second[:, :key_cols],
        new_first[:, key_cols:],
        new_second[:, key_cols:],
    )


def solution(mesh):
    placed = (
        P("fs", None),
        P("fs", "tp"),
        P("fs", "tp"),
        P("fs", None),
        P("fs", "tp"),
        P("fs", "tp"),
        P("fs", "tp"),
        P("fs", "tp"),
        P("fs", "tp"),
        P("fs", "tp"),
    )
    return jax.shard_map(
        on_device,
        mesh=mesh,
        in_specs=placed,
        out_specs=(
            P("fs", "tp"),
            P("fs", "tp"),
            P("fs", "tp"),
            P("fs", "tp"),
            P(None, "tp"),
            P(None, "tp"),
            P("fs", "tp"),
            P("fs", "tp"),
            P("fs", "tp"),
            P("fs", "tp"),
        ),
        check_vma=False,
    )
```

profile of v0, /device:TPU:0, one launch (start us, length us, event | category | flops | bytes accessed | tf_op | source)
XLA Modules:
  0.0 406.0 jit_solution(744935510458757411)
XLA Ops:
  7.2 0.0 all-gather.4.cloned.1.call-start
  7.2 0.7 all-gather.4.cloned.1.call-update
  7.9 0.0 all-reduce.2.cloned.1.call-start
  8.0 0.0 copy-start
  8.0 1.4 constant_dynamic-update-slice_fusion.1
  9.4 0.5 copy-done
  9.9 0.2 constant_dynamic-update-slice_fusion
  10.0 58.5 %all-gather.4.cloned.1.call-done = bf16[2048,256]{1,0:T(8,128)(2,1)} async-done(((bf16[128,256]{1,0:T(8,128)(2,1)}), bf16[2048,256]{1,0:T(8,128)(2,1)}) %all-gather.4.cloned.1.call-update) | async-done | bytes 1048592 | tf_op jit(solution)/shard_map/all_gather | solution.py:33
  68.6 3.7 fusion.6
  72.3 1.0 fusion.1
  73.4 0.0 copy-start.2
  73.4 2.2 convolution_add_fusion
  75.5 0.0 copy-start.3
  75.5 0.0 copy-start.4
  75.5 0.0 copy-start.5
  75.5 0.0 copy-start.6
  75.5 0.0 copy-start.1
  75.6 0.0 all-reduce.2.cloned.1.call-update
  75.6 0.0 all-gather.6.cloned.1.call-start
  75.6 0.0 copy-done.2
  75.7 0.1 copy.20
  75.8 1.2 copy.21
  77.0 115.1 %all-reduce.2.cloned.1.call-done = f32[256,1536]{1,0:T(8,128)} async-done(((f32[256,1536]{1,0:T(8,128)}), f32[256,1536]{1,0:T(8,128)}) %all-reduce.2.cloned.1.call-update) | async-done | bytes 1572880 | tf_op jit(solution)/shard_map/psum | solution.py:44
  192.1 2.4 multiply_reduce_fusion
  194.5 3.1 psum.15
  198.3 0.0 copy-done.3
  198.3 0.0 copy-done.4
  198.3 0.0 copy-done.5
  198.3 0.0 copy-done.6
  198.3 1.0 divide_convert_fusion
  199.3 43.7 %all_gather.13 = bf16[256,1536]{1,0:T(8,128)(2,1)S(1)} all-gather(bf16[16,1536]{1,0:T(8,128)(2,1)S(1)} %get-tuple-element.22), channel_id=1, replica_groups=mesh['fs'=16,'tp'=2] {'fs'}, dimensions={0}, use_global_device_ids=true | all-gather | bytes 835584 | tf_op jit(solution)/shard_map/all_gather | solution.py:55
  243.0 0.0 copy-done.1
  243.0 0.4 fusion.4
  243.4 0.7 slice.44
  244.1 0.0 all-gather.6.cloned.1.call-update
  244.1 0.0 all-gather.8.cloned.1.call-start
  244.1 0.7 slice.45
  244.9 0.0 all-gather.8.cloned.1.call-update
  244.9 0.6 slice.47
  245.5 0.6 slice.49
  246.1 0.6 slice.46
  246.7 0.6 slice.48
  247.5 1.0 copy.25
  248.5 0.8 copy.24
  249.4 1.0 copy.23
  250.3 0.8 copy.22
  251.2 51.9 %all-gather.6.cloned.1.call-done = bf16[2048,512]{0,1:T(8,128)(2,1)} async-done(((bf16[128,512]{0,1:T(8,128)(2,1)}), bf16[2048,512]{0,1:T(8,128)(2,1)}) %all-gather.6.cloned.1.call-update) | async-done | bytes 2097168 | tf_op jit(solution)/shard_map/all_gather | solution.py:61
  303.0 3.9 copy.26
  307.0 86.1 %all-gather.8.cloned.1.call-done = bf16[2048,1024]{0,1:T(8,128)(2,1)} async-done(((bf16[128,1024]{0,1:T(8,128)(2,1)}), bf16[2048,1024]{0,1:T(8,128)(2,1)}) %all-gather.8.cloned.1.call-update) | async-done | bytes 4194320 | tf_op jit(solution)/shard_map/all_gather | solution.py:62
  393.1 6.4 %copy.27 = bf16[2048,1024]{1,0:T(8,128)(2,1)} copy(bf16[2048,1024]{0,1:T(8,128)(2,1)} %all-gather.8.cloned.1.call-done) | data formatting | bytes 8388608
  (4 shorter events, 0.1 us)
Async XLA Ops:
  7.2 61.4 %all-gather.4.cloned.1.call-start = ((), (), s32[]{:S(2)}) async-start(), calls=%async_computation | async-start | bytes 1114112 | tf_op jit(solution)/shard_map/all_gather | solution.py:33
  7.9 184.2 %all-reduce.2.cloned.1.call-start = ((), (), s32[]{:S(2)}) async-start(), calls=%async_computation.1 | async-start | bytes 3145728 | tf_op jit(solution)/shard_map/psum | solution.py:44
  8.0 1.9 copy-start
  73.4 2.3 copy-start.2
  75.5 122.7 %copy-start.3 = (f32[16,1024]{1,0:T(8,128)S(1)}, f32[16,1024]{1,0:T(8,128)}, u32[]{:S(2)}) copy-start(f32[16,1024]{1,0:T(8,128)} %param.19) | copy-start | bytes 196612
  75.5 122.8 %copy-start.4 = (f32[16,1024]{1,0:T(8,128)S(1)}, f32[16,1024]{1,0:T(8,128)}, u32[]{:S(2)}) copy-start(f32[16,1024]{1,0:T(8,128)} %param.18) | copy-start | bytes 196612
  75.5 122.8 %copy-start.5 = (f32[16,512]{1,0:T(8,128)S(1)}, f32[16,512]{1,0:T(8,128)}, u32[]{:S(2)}) copy-start(f32[16,512]{1,0:T(8,128)} %param.17) | copy-start | bytes 98308
  75.5 122.8 %copy-start.6 = (f32[16,512]{1,0:T(8,128)S(1)}, f32[16,512]{1,0:T(8,128)}, u32[]{:S(2)}) copy-start(f32[16,512]{1,0:T(8,128)} %param.16) | copy-start | bytes 98308
  75.5 167.4 %copy-start.1 = (bf16[128,256]{1,0:T(8,128)(2,1)S(1)}, bf16[128,256]{1,0:T(8,128)(2,1)}, u32[]{:S(2)}) copy-start(bf16[128,256]{1,0:T(8,128)(2,1)} %param.13) | copy-start | bytes 196612
  75.6 227.5 %all-gather.6.cloned.1.call-start = ((), (), s32[]{:S(2)}) async-start(), calls=%async_computation.2 | async-start | bytes 2228224 | tf_op jit(solution)/shard_map/all_gather | solution.py:61
  244.1 149.0 %all-gather.8.cloned.1.call-start = ((), (), s32[]{:S(2)}) async-start(), calls=%async_computation.3 | async-start | bytes 4456448 | tf_op jit(solution)/shard_map/all_gather | solution.py:62
Sparse Core Ops, SparseCore 0:
  10.7 57.7 all-gather.3
  75.7 116.3 all-reduce.1
  244.2 58.7 all-gather.5
  306.2 86.8 all-gather.7
where the time goes:
time: 406 us
  waiting for transfers between devices  312 us (77%)
  blocking collectives  46.8 us (12%)
  local copies, waits for them, and re-layouts  21.4 us (5%)
  between operations  14.6 us (4%)
  matrix products  7.34 us (2%)
    psum x1, waiting for transfers between devices, on_device(): summed = lax.psum(partial_value, 'fs')  115 us
    all_gather x1, waiting for transfers between devices, on_device(): lax.all_gather(half_copy[:, key_cols:], 'fs', axis=0, tiled=True)  86.1 us
    all_gather x1, waiting for transfers between devices, on_device(): lax.all_gather(basis, 'fs', axis=0, tiled=True)  58.5 us
    all_gather x1, waiting for transfers between devices, on_device(): lax.all_gather(half_copy[:, :key_cols], 'fs', axis=0, tiled=True)  51.9 us
    all_gather x1, blocking collectives, on_device(): all_directions = lax.all_gather(direction, 'fs', axis=0, tiled=True)  43.7 us
    unnamed x23, local copies, waits for them, and re-layouts  17.3 us
  transfers between devices with their start and end apart: 4, of which 4 were waited for; matrix products, arithmetic and copies ran while one was open for 3% of the time, Pallas kernels for 0%

commit v1 on v0

v1 whole, which is shorter than its diff:
```python
import functools

import jax
import jax.numpy as jnp
from jax import lax
from jax.experimental import pallas as pl
from jax.experimental.pallas import tpu as pltpu
from jax.sharding import PartitionSpec as P

learn_rate = 0.05
beta_first = 0.9
beta_second = 0.9
epsilon = 1e-08
norm_eps = 1e-06

MESH = pl.DeviceIdType.MESH
F32 = jnp.float32
BF16 = jnp.bfloat16


class Gather:
    def __init__(self, lines, slot, own, send_sem, recv_sem):
        self.lines, self.slot, self.own = lines, slot, own
        self.send_sem, self.recv_sem = send_sem, recv_sem
        self.me = lax.axis_index("fs")
        self.z = self.me // 4
        self.y = lax.rem(self.me // 2, 2)
        self.x = lax.rem(self.me, 2)
        self.sent = []

    def at(self, i, fy, fx):
        y = 1 - self.y if fy else self.y
        x = 1 - self.x if fx else self.x
        return lax.rem(self.z - i + self.lines, self.lines) * 4 + y * 2 + x

    def send(self, part, index, source, owner, target):
        copy = pltpu.make_async_remote_copy(
            src_ref=source,
            dst_ref=self.slot(owner, part),
            send_sem=self.send_sem.at[part, index],
            recv_sem=self.recv_sem.at[part, index],
            device_id={"fs": target},
            device_id_type=MESH,
        )
        copy.start()
        self.sent.append(copy)

    def arrive(self, part, index, owner):
        place = self.slot(owner, part)
        pltpu.make_async_remote_copy(
            src_ref=place,
            dst_ref=place,
            send_sem=self.send_sem.at[part, index],
            recv_sem=self.recv_sem.at[part, index],
            device_id={"fs": self.at(0, 0, 1)},
            device_id_type=MESH,
        ).wait_recv()

    def flips(self, part):
        return ((1, 0), (0, 1)) if part == 0 else ((0, 1), (1, 0))

    def along_z(self):
        for part in range(2):
            for k in range(1, self.lines):
                self.send(part, k, self.own(part), self.me, self.at(self.lines - k, 0, 0))

    def hop_one(self, part, i):
        first, _ = self.flips(part)
        owner = self.at(i, 0, 0)
        source = self.own(part) if i == 0 else self.slot(owner, part)
        self.send(part, self.lines + i, source, owner, self.at(0, *first))

    def hop_two(self, part, i, flipped):
        first, second = self.flips(part)
        owner = self.at(i, *first) if flipped else self.at(i, 0, 0)
        source = self.own(part) if i == 0 and not flipped else self.slot(owner, part)
        self.send(part, (3 if flipped else 2) * self.lines + i, source, owner, self.at(0, *second))

    def steps(self):
        def begin():
            for part in range(2):
                self.hop_one(part, 0)
            for part in range(2):
                self.hop_two(part, 0, False)

        def from_line(i):
            for part in range(2):
                self.arrive(part, i, self.at(i, 0, 0))
                self.hop_one(part, i)
            for part in range(2):
                self.hop_two(part, i, False)

        def from_first(i):
            for part in range(2):
                first, _ = self.flips(part)
                self.arrive(part, self.lines + i, self.at(i, *first))
                self.hop_two(part, i, True)

        def from_second(i):
            for part in range(2):
                first, second = self.flips(part)
                self.arrive(part, 2 * self.lines + i, self.at(i, *second))
                self.arrive(part, 3 * self.lines + i, self.at(i, 1, 1))

        out = [begin]
        for i in range(1, self.lines):
            out.append(functools.partial(from_line, i))
            out.append(functools.partial(from_first, i - 1))
        out.append(functools.partial(from_first, self.lines - 1))
        tail = [functools.partial(from_second, i) for i in range(self.lines)]
        return out, tail

    def close(self):
        for copy in self.sent:
            copy.wait_send()


def exchange_kernel(
    n,
    tp,
    count,
    normed,
    key_cot,
    value_cot,
    basis,
    master,
    first_key,
    second_key,
    first_value,
    second_value,
    basis_all,
    master_all,
    dirs_all,
    new_first_key,
    new_second_key,
    new_first_value,
    new_second_value,
    normed_v,
    key_v,
    value_v,
    projected,
    partial,
    received,
    direction,
    own_square,
    squares,
    chip_square,
    chip_squares,
    load_sem,
    basis_send,
    basis_recv,
    master_send,
    master_recv,
    dirs_send,
    dirs_recv,
    part_send,
    part_recv,
    square_send,
    square_recv,
    chip_send,
    chip_recv,
):
    me = lax.axis_index("fs")
    my_tp = lax.axis_index("tp")
    loads = [
        pltpu.make_async_copy(source, target, load_sem.at[i])
        for i, (source, target) in enumerate(((normed, normed_v), (key_cot, key_v), (value_cot, value_v)))
    ]
    for load in loads:
        load.start()

    barrier = pltpu.get_barrier_semaphore()
    for k in range(1, n):
        pl.semaphore_signal(barrier, inc=1, device_id={"fs": lax.rem(me + k, n)}, device_id_type=MESH)
    for k in range(1, tp):
        pl.semaphore_signal(barrier, inc=1, device_id={"tp": lax.rem(my_tp + k, tp)}, device_id_type=MESH)
    pl.semaphore_wait(barrier, n - 1 + tp - 1)

    lines = n // 4

    def gather(whole, own, send_sem, recv_sem, stacked):
        cols = own.shape[-1]
        cut = cols // 256 * 128
        spans = (pl.ds(0, cut), pl.ds(cut, cols - cut))
        rows = own.shape[0]

        def slot(owner, part):
            if stacked:
                return whole.at[owner, :, spans[part]]
            return whole.at[pl.ds(pl.multiple_of(owner * rows, rows), rows), spans[part]]

        return Gather(lines, slot, lambda part: own.at[:, spans[part]], send_sem, recv_sem)

    basis_g = gather(basis_all, basis, basis_send, basis_recv, False)
    master_g = gather(master_all, master, master_send, master_recv, False)
    dirs_g = gather(dirs_all, direction, dirs_send, dirs_recv, True)

    basis_g.along_z()
    steps, tail = basis_g.steps()
    steps[0]()
    master_g.along_z()
    rows = basis.shape[0]
    own_rows = pl.ds(pl.multiple_of(me * rows, rows), rows)
    basis_all[own_rows, :] = basis[...]
    master_all[own_rows, :] = master[...]
    for step in steps[1:]:
        step()
    master_steps, master_tail = master_g.steps()
    master_steps[0]()
    for step in tail:
        step()

    loads[0].wait()
    tokens = normed_v.shape[0]
    tile = 256

    @pl.loop(0, tokens // tile)
    def _(t):
        at = pl.ds(pl.multiple_of(t * tile, tile), tile)
        projected[at, :] = jnp.dot(normed_v[at, :], basis_all[...], preferred_element_type=F32).astype(BF16)

    loads[1].wait()
    loads[2].wait()
    kc = key_v.shape[1]
    rank_rows = first_key.shape[0]

    def project(cot, base):
        width = cot.shape[1]
        step = min(width, 512)
        for c in range(0, width, step):
            sums = lax.dot_general(
                projected[...], cot[:, c : c + step], (((0,), (0,)), ((), ())), preferred_element_type=F32
            ).astype(BF16)
            for j in range(n):
                partial[j, :, base + c : base + c + step] = sums[j * rank_rows : (j + 1) * rank_rows, :]

    project(key_v, 0)
    project(value_v, kc)

    part_copies = []
    for k in range(1, n):
        target = lax.rem(me + k, n)
        copy = pltpu.make_async_remote_copy(
            src_ref=partial.at[target],
            dst_ref=received.at[k],
            send_sem=part_send.at[k],
            recv_sem=part_recv.at[k],
            device_id={"fs": target},
            device_id_type=MESH,
        )
        copy.start()
        part_copies.append(copy)
    low = partial[me].astype(F32)
    received[0] = partial[me]
    for step in master_steps[1:]:
        step()
    for k, copy in enumerate(part_copies):
        copy.wait_recv()
    low = received[0].astype(F32)
    for k in range(1, n):
        low = low + received[k].astype(F32)

    square = jnp.sum(low * low)
    own_square[...] = jnp.full(own_square.shape, square, F32)
    squares[0] = jnp.full(own_square.shape, square, F32)
    square_copies = []
    for k in range(1, n):
        copy = pltpu.make_async_remote_copy(
            src_ref=own_square,
            dst_ref=squares.at[k],
            send_sem=square_send.at[k],
            recv_sem=square_recv.at[k],
            device_id={"fs": lax.rem(me + k, n)},
            device_id_type=MESH,
        )
        copy.start()
        square_copies.append(copy)
    for copy in square_copies:
        copy.wait_recv()
    chip_square[...] = jnp.sum(squares[...], axis=0)
    chip_squares[0] = jnp.sum(squares[...], axis=0)
    chip_copies = []
    for k in range(1, tp):
        copy = pltpu.make_async_remote_copy(
            src_ref=chip_square,
            dst_ref=chip_squares.at[k],
            send_sem=chip_send.at[k],
            recv_sem=chip_recv.at[k],
            device_id={"tp": lax.rem(my_tp + k, tp)},
            device_id_type=MESH,
        )
        copy.start()
        chip_copies.append(copy)
    for copy in chip_copies:
        copy.wait_recv()
    total = jnp.sum(chip_squares[...], axis=0)[0:1, 0:1]
    grad_scale = 1.0 / jnp.sqrt(total / count + norm_eps)

    def update(scaled, first, second, new_first, new_second, base):
        moved = beta_first * first[...] + (1.0 - beta_first) * scaled
        spread = beta_second * second[...] + (1.0 - beta_second) * scaled * scaled
        new_first[...] = moved
        new_second[...] = spread
        turned = (moved / (jnp.sqrt(spread) + epsilon)).astype(BF16)
        direction[:, base : base + turned.shape[1]] = turned
        dirs_all[me, :, base : base + turned.shape[1]] = turned

    scaled = low * grad_scale
    update(scaled[:, :kc], first_key, second_key, new_first_key, new_second_key, 0)
    update(scaled[:, kc:], first_value, second_value, new_first_value, new_second_value, kc)

    dirs_g.along_z()
    dirs_steps, dirs_tail = dirs_g.steps()
    for step in dirs_steps + dirs_tail + master_tail:
        step()
    for g in (basis_g, master_g, dirs_g):
        g.close()
    for copy in part_copies + square_copies + chip_copies:
        copy.wait_send()


def final_kernel(basis_all, master_all, dirs, basis, master_key, master_value, copy_key, copy_value, step_key, step_value, new_key, new_value):
    kc = copy_key.shape[1]
    for cut, out in ((slice(0, kc), copy_key), (slice(kc, None), copy_value)):
        step = jnp.dot(basis_all[...], dirs[:, cut], preferred_element_type=F32)
        out[...] = (master_all[:, cut].astype(F32) - learn_rate * step).astype(BF16)

    @pl.when(pl.program_id(0) == 0)
    def _():
        for cut, master, step_out, new in (
            (slice(0, kc), master_key, step_key, new_key),
            (slice(kc, None), master_value, step_value, new_value),
        ):
            step = jnp.dot(basis[...], dirs[:, cut], preferred_element_type=F32)
            step_out[...] = step
            new[...] = master[...] - learn_rate * step


def on_device(
    n,
    tp,
    normed,
    key_cot,
    value_cot,
    basis,
    master_key,
    master_value,
    first_key,
    second_key,
    first_value,
    second_value,
):
    rows, rank = basis.shape
    d = rows * n
    kc, vc = key_cot.shape[1], value_cot.shape[1]
    cols = kc + vc
    tokens = normed.shape[0]
    rank_rows = first_key.shape[0]
    lines = n // 4
    master = jnp.concatenate([master_key.astype(BF16), master_value.astype(BF16)], axis=1)
    vmem = pl.BlockSpec(memory_space=pltpu.VMEM)
    hbm = pl.BlockSpec(memory_space=pl.ANY)
    dma = pltpu.SemaphoreType.DMA
    small = (8, 128)
    basis_all, master_all, dirs, nfk, nsk, nfv, nsv = pl.pallas_call(
        functools.partial(exchange_kernel, n, tp, rank * cols * tp),
        out_shape=(
            jax.ShapeDtypeStruct((d, rank), BF16),
            jax.ShapeDtypeStruct((d, cols), BF16),
            jax.ShapeDtypeStruct((n, rank_rows, cols), BF16),
            jax.ShapeDtypeStruct(first_key.shape, F32),
            jax.ShapeDtypeStruct(first_key.shape, F32),
            jax.ShapeDtypeStruct(first_value.shape, F32),
            jax.ShapeDtypeStruct(first_value.shape, F32),
        ),
        in_specs=[hbm] * 3 + [vmem] * 6,
        out_specs=[vmem] * 7,
        scratch_shapes=[
            pltpu.VMEM(normed.shape, BF16),
            pltpu.VMEM(key_cot.shape, BF16),
            pltpu.VMEM(value_cot.shape, BF16),
            pltpu.VMEM((tokens, rank), BF16),
            pltpu.VMEM((n, rank_rows, cols), BF16),
            pltpu.VMEM((n, rank_rows, cols), BF16),
            pltpu.VMEM((rank_rows, cols), BF16),
            pltpu.VMEM(small, F32),
            pltpu.VMEM((n, *small), F32),
            pltpu.VMEM(small, F32),
            pltpu.VMEM((tp, *small), F32),
            dma((3,)),
        ]
        + [dma((2, 4 * lines))] * 6
        + [dma((n,))] * 4
        + [dma((tp,))] * 2,
        compiler_params=pltpu.CompilerParams(
            collective_id=0, has_side_effects=True, vmem_limit_bytes=50 * 1024 * 1024
        ),
    )(normed, key_cot, value_cot, basis, master, first_key, second_key, first_value, second_value)
    dirs = dirs.reshape(rank, cols)

    block = 256
    whole = lambda *shape: pl.BlockSpec(shape, lambda i: (0,) * len(shape))
    sliced = lambda width: pl.BlockSpec((block, width), lambda i: (i, 0))
    copy_key, copy_value, step_key, step_value, new_key, new_value = pl.pallas_call(
        final_kernel,
        grid=(d // block,),
        out_shape=(
            jax.ShapeDtypeStruct((d, kc), BF16),
            jax.ShapeDtypeStruct((d, vc), BF16),
            jax.ShapeDtypeStruct((rows, kc), F32),
            jax.ShapeDtypeStruct((rows, vc), F32),
            jax.ShapeDtypeStruct((rows, kc), F32),
            jax.ShapeDtypeStruct((rows, vc), F32),
        ),
        in_specs=[
            sliced(rank),
            sliced(cols),
            whole(rank, cols),
            whole(rows, rank),
            whole(rows, kc),
            whole(rows, vc),
        ],
        out_specs=[sliced(kc), sliced(vc), whole(rows, kc), whole(rows, vc), whole(rows, kc), whole(rows, vc)],
    )(basis_all, master_all, dirs, basis, master_key, master_value)
    return (step_key, step_value, new_key, new_value, copy_key, copy_value, nfk, nsk, nfv, nsv)


def solution(mesh):
    split = P("fs", "tp")
    lone = P("fs", None)
    return jax.shard_map(
        functools.partial(on_device, mesh.shape["fs"], mesh.shape["tp"]),
        mesh=mesh,
        in_specs=(lone, split, split, lone) + (split,) * 6,
        out_specs=(split,) * 4 + (P(None, "tp"),) * 2 + (split,) * 4,
        check_vma=False,
    )
```

time: 406 us -> 134 us (0.33)
  waiting for transfers between devices: 312 us -> 0 us
  Pallas kernels: 0 us -> 121 us
  blocking collectives: 46.8 us -> 0 us
  between operations: 14.6 us -> 0.7 us
  local copies, waits for them, and re-layouts: 21.4 us -> 9.6 us
  matrix products: 7.34 us -> 0 us
    all_gather x3 -> x0, waiting for transfers between devices: 197 us -> none  [the longest x1 86.1 us: on_device(): lax.all_gather(half_copy[:, key_cols:], 'fs', axis=0, tiled=True)]
    pallas_call x0 -> x2, Pallas kernels: none -> 121 us  [the longest x1 110 us: on_device(): pl.pallas_call(functools.partial(exchange_kernel, n, tp, rank * cols * tp...]
    psum x1 -> x0, waiting for transfers between devices: 115 us -> none  [on_device(): summed = lax.psum(partial_value, 'fs')]
    all_gather x1 -> x0, blocking collectives: 43.7 us -> none  [on_device(): all_directions = lax.all_gather(direction, 'fs', axis=0, tiled=True)]
    unnamed x23 -> x20, local copies, waits for them, and re-layouts: 17.3 us -> 9.6 us
    dot_general x4 -> x0, matrix products: 7.34 us -> none  [the longest x1 3.74 us: on_device(): jnp.dot(normed, lax.all_gather(basis, 'fs', axis=0, tiled=True), preferre...]
  transfers between devices with their start and end apart: 4 -> 0, of which waited for: 4 -> 0; matrix products, arithmetic and copies ran while one was open for 3% -> 0% of each run, Pallas kernels for 0% -> 0%
where the time goes in v1:
time: 134 us; the launch traced here: 133 us
  Pallas kernels  121 us (90%)
  local copies, waits for them, and re-layouts  9.6 us (7%)
  other arithmetic  2.07 us (2%)
    pallas_call x1, Pallas kernels, on_device(): pl.pallas_call(functools.partial(exchange_kernel, n, tp, rank * cols * tp...  110 us
    pallas_call x1, Pallas kernels, on_device(): pl.pallas_call(final_kernel, grid=(d // block,), out_shape=(jax.ShapeDtyp...  10.6 us
    unnamed x20, local copies, waits for them, and re-layouts  9.6 us

profile of v1, /device:TPU:0, one launch (start us, length us, event | category | flops | bytes accessed | tf_op | source)
XLA Modules:
  0.0 133.4 jit_solution(3219702119638053608)
XLA Ops:
  0.6 1.0 convert_element_type.6
  1.6 1.1 convert_element_type.7
  2.7 0.0 copy-start
  2.7 1.2 copy-done
  4.0 0.0 copy-start.3
  4.0 0.8 copy-done.3
  4.8 0.0 copy-start.4
  4.8 0.8 copy-done.4
  5.6 0.0 copy-start.5
  5.6 0.8 copy-done.5
  6.5 0.0 copy-start.6
  6.5 0.8 copy-done.6
  7.2 0.0 copy-start.7
  7.2 0.8 copy-done.7
  8.0 110.5 %shard_map.177 = (bf16[2048,256]{1,0:T(8,128)(2,1)S(1)}, bf16[2048,1536]{1,0:T(8,128)(2,1)}, bf16[16,16,1536]{2,1,0:T(8,128)(2,1)S(1)}, f32[16,512]{1,0:T(8,128)...) custom-call(bf16[1024,2048]{1,0:T(8,128)(2,1)} %normed.1, ...), custom_call_target="tpu_custom_call" | custom-call | tf_op jit(solution)/shard_map/pallas_call | solution.py:365
  118.5 0.0 copy-start.1
  118.5 1.0 copy-done.1
  119.4 0.0 copy-start.2
  119.4 0.9 copy-done.2
  120.3 10.6 %shard_map.178 = (bf16[2048,512]{1,0:T(8,128)(2,1)}, bf16[2048,1024]{1,0:T(8,128)(2,1)}, f32[128,512]{1,0:T(8,128)}, f32[128,1024]{1,0:T(8,128)}, f32[128,512]{1,0:T(8,128)}, /*index=5*/f32[128,1024]{1,0:T(8,128)}) custom-call(bf16[2048,256]{1,0:T(8,128)(2,1)} %copy-done.1, bf16[2048,1536]{1,0:T(8,128)(2,1)} %get-tuple-element.24.master_all, ...), custom_call_target="tpu_custom_call" | custom-call | tf_op jit(solution)/shard_map/pallas_call | solution.py:404
  131.0 0.6 copy.24
  131.6 0.6 copy.25
  132.2 0.6 copy.26
  132.8 0.6 copy.27
  (1 shorter events, 0.0 us)
Async XLA Ops:
  2.7 1.2 copy-start
  4.0 0.8 copy-start.3
  4.8 0.8 copy-start.4
  5.6 0.8 copy-start.5
  6.5 0.8 copy-start.6
  7.2 0.8 copy-start.7
  118.5 1.0 copy-start.1
  119.4 0.9 copy-start.2

commit v2 on v1

--- a/solution.py
+++ b/solution.py
@@ -12,6 +12,8 @@
 beta_second = 0.9
 epsilon = 1e-08
 norm_eps = 1e-06
+
+SHARES = (16, 16, 16)
 
 MESH = pl.DeviceIdType.MESH
 F32 = jnp.float32
@@ -26,12 +28,21 @@
         self.z = self.me // 4
         self.y = lax.rem(self.me // 2, 2)
         self.x = lax.rem(self.me, 2)
+        self.along = [self.partner(i) for i in range(lines)]
         self.sent = []
+
+    def partner(self, i):
+        out, bit = self.z, 1
+        while bit <= i:
+            if i & bit:
+                out = out + bit - 2 * bit * lax.rem(self.z // bit, 2)
+            bit *= 2
+        return out
 
     def at(self, i, fy, fx):
         y = 1 - self.y if fy else self.y
         x = 1 - self.x if fx else self.x
-        return lax.rem(self.z - i + self.lines, self.lines) * 4 + y * 2 + x
+        return self.along[i] * 4 + y * 2 + x
 
     def send(self, part, index, source, owner, target):
         copy = pltpu.make_async_remote_copy(
@@ -59,10 +70,10 @@
     def flips(self, part):
         return ((1, 0), (0, 1)) if part == 0 else ((0, 1), (1, 0))
 
-    def along_z(self):
-        for part in range(2):
-            for k in range(1, self.lines):
-                self.send(part, k, self.own(part), self.me, self.at(self.lines - k, 0, 0))
+    def along_z(self, start=1, stop=None):
+        for k in range(start, stop or self.lines):
+            for part in range(2):
+                self.send(part, k, self.own(part), self.me, self.at(k, 0, 0))
 
     def hop_one(self, part, i):
         first, _ = self.flips(part)
@@ -122,22 +133,28 @@
     normed,
     key_cot,
     value_cot,
+    basis_in,
+    master_key,
+    master_value,
+    first_key_in,
+    second_key_in,
+    first_value_in,
+    second_value_in,
+    basis_all,
+    master_all,
+    dirs_all,
+    scaled_out,
+    normed_v,
+    key_v,
+    value_v,
     basis,
-    master,
+    master_key_v,
+    master_value_v,
     first_key,
     second_key,
     first_value,
     second_value,
-    basis_all,
-    master_all,
-    dirs_all,
-    new_first_key,
-    new_second_key,
-    new_first_value,
-    new_second_value,
-    normed_v,
-    key_v,
-    value_v,
+    master,
     projected,
     partial,
     received,
@@ -164,7 +181,20 @@
     my_tp = lax.axis_index("tp")
     loads = [
         pltpu.make_async_copy(source, target, load_sem.at[i])
-        for i, (source, target) in enumerate(((normed, normed_v), (key_cot, key_v), (value_cot, value_v)))
+        for i, (source, target) in enumerate(
+            (
+                (basis_in, basis),
+                (master_key, master_key_v),
+                (master_value, master_value_v),
+                (normed, normed_v),
+                (key_cot, key_v),
+                (value_cot, value_v),
+                (first_key_in, first_key),
+                (second_key_in, second_key),
+                (first_value_in, first_value),
+                (second_value_in, second_value),
+            )
+        )
     ]
     for load in loads:
         load.start()
@@ -195,10 +225,17 @@
     master_g = gather(master_all, master, master_send, master_recv, False)
     dirs_g = gather(dirs_all, direction, dirs_send, dirs_recv, True)
 
+    loads[0].wait()
     basis_g.along_z()
     steps, tail = basis_g.steps()
     steps[0]()
-    master_g.along_z()
+    loads[1].wait()
+    loads[2].wait()
+    cut = master_key_v.shape[1]
+    master[:, :cut] = master_key_v[...].astype(BF16)
+    master[:, cut:] = master_value_v[...].astype(BF16)
+    early = lines
+    master_g.along_z(1, early)
     rows = basis.shape[0]
     own_rows = pl.ds(pl.multiple_of(me * rows, rows), rows)
     basis_all[own_rows, :] = basis[...]
@@ -210,7 +247,7 @@
     for step in tail:
         step()
 
-    loads[0].wait()
+    loads[3].wait()
     tokens = normed_v.shape[0]
     tile = 256
 
@@ -219,8 +256,8 @@
         at = pl.ds(pl.multiple_of(t * tile, tile), tile)
         projected[at, :] = jnp.dot(normed_v[at, :], basis_all[...], preferred_element_type=F32).astype(BF16)
 
-    loads[1].wait()
-    loads[2].wait()
+    loads[4].wait()
+    loads[5].wait()
     kc = key_v.shape[1]
     rank_rows = first_key.shape[0]
 
@@ -252,7 +289,9 @@
         part_copies.append(copy)
     low = partial[me].astype(F32)
     received[0] = partial[me]
-    for step in master_steps[1:]:
+    master_g.along_z(early, lines)
+    turns = [len(master_steps) * part // 16 for part in SHARES]
+    for step in master_steps[1 : turns[0]]:
         step()
     for k, copy in enumerate(part_copies):
         copy.wait_recv()
@@ -275,6 +314,8 @@
         )
         copy.start()
         square_copies.append(copy)
+    for step in master_steps[turns[0] : turns[1]]:
+        step()
     for copy in square_copies:
         copy.wait_recv()
     chip_square[...] = jnp.sum(squares[...], axis=0)
@@ -296,22 +337,26 @@
     total = jnp.sum(chip_squares[...], axis=0)[0:1, 0:1]
     grad_scale = 1.0 / jnp.sqrt(total / count + norm_eps)
 
-    def update(scaled, first, second, new_first, new_second, base):
+    def update(scaled, first, second, base):
         moved = beta_first * first[...] + (1.0 - beta_first) * scaled
         spread = beta_second * second[...] + (1.0 - beta_second) * scaled * scaled
-        new_first[...] = moved
-        new_second[...] = spread
         turned = (moved / (jnp.sqrt(spread) + epsilon)).astype(BF16)
         direction[:, base : base + turned.shape[1]] = turned
         dirs_all[me, :, base : base + turned.shape[1]] = turned
 
+    for load in loads[6:]:
+        load.wait()
     scaled = low * grad_scale
-    update(scaled[:, :kc], first_key, second_key, new_first_key, new_second_key, 0)
-    update(scaled[:, kc:], first_value, second_value, new_first_value, new_second_value, kc)
+    scaled_out[...] = scaled
+    update(scaled[:, :kc], first_key, second_key, 0)
+    update(scaled[:, kc:], first_value, second_value, kc)
 
     dirs_g.along_z()
     dirs_steps, dirs_tail = dirs_g.steps()
-    for step in dirs_steps + dirs_tail + master_tail:
+    dirs_steps[0]()
+    for step in master_steps[turns[1] : turns[2]] + dirs_steps[1:] + master_steps[turns[2] :]:
+        step()
+    for step in dirs_tail + master_tail:
         step()
     for g in (basis_g, master_g, dirs_g):
         g.close()
@@ -319,7 +364,29 @@
         copy.wait_send()
 
 
-def final_kernel(basis_all, master_all, dirs, basis, master_key, master_value, copy_key, copy_value, step_key, step_value, new_key, new_value):
+def final_kernel(
+    basis_all,
+    master_all,
+    dirs,
+    basis,
+    master_key,
+    master_value,
+    scaled,
+    first_key,
+    second_key,
+    first_value,
+    second_value,
+    copy_key,
+    copy_value,
+    step_key,
+    step_value,
+    new_key,
+    new_value,
+    new_first_key,
+    new_second_key,
+    new_first_value,
+    new_second_value,
+):
     kc = copy_key.shape[1]
     for cut, out in ((slice(0, kc), copy_key), (slice(kc, None), copy_value)):
         step = jnp.dot(basis_all[...], dirs[:, cut], preferred_element_type=F32)
@@ -334,6 +401,13 @@
             step = jnp.dot(basis[...], dirs[:, cut], preferred_element_type=F32)
             step_out[...] = step
             new[...] = master[...] - learn_rate * step
+        for cut, first, second, new_first, new_second in (
+            (slice(0, kc), first_key, second_key, new_first_key, new_second_key),
+            (slice(kc, None), first_value, second_value, new_first_value, new_second_value),
+        ):
+            own = scaled[:, cut]
+            new_first[...] = beta_first * first[...] + (1.0 - beta_first) * own
+            new_second[...] = beta_second * second[...] + (1.0 - beta_second) * own * own
 
 
 def on_device(
@@ -357,28 +431,32 @@
     tokens = normed.shape[0]
     rank_rows = first_key.shape[0]
     lines = n // 4
-    master = jnp.concatenate([master_key.astype(BF16), master_value.astype(BF16)], axis=1)
     vmem = pl.BlockSpec(memory_space=pltpu.VMEM)
     hbm = pl.BlockSpec(memory_space=pl.ANY)
     dma = pltpu.SemaphoreType.DMA
     small = (8, 128)
-    basis_all, master_all, dirs, nfk, nsk, nfv, nsv = pl.pallas_call(
+    basis_all, master_all, dirs, scaled = pl.pallas_call(
         functools.partial(exchange_kernel, n, tp, rank * cols * tp),
         out_shape=(
             jax.ShapeDtypeStruct((d, rank), BF16),
             jax.ShapeDtypeStruct((d, cols), BF16),
             jax.ShapeDtypeStruct((n, rank_rows, cols), BF16),
-            jax.ShapeDtypeStruct(first_key.shape, F32),
-            jax.ShapeDtypeStruct(first_key.shape, F32),
-            jax.ShapeDtypeStruct(first_value.shape, F32),
-            jax.ShapeDtypeStruct(first_value.shape, F32),
+            jax.ShapeDtypeStruct((rank_rows, cols), F32),
         ),
-        in_specs=[hbm] * 3 + [vmem] * 6,
-        out_specs=[vmem] * 7,
+        in_specs=[hbm] * 10,
+        out_specs=[vmem] * 4,
         scratch_shapes=[
             pltpu.VMEM(normed.shape, BF16),
             pltpu.VMEM(key_cot.shape, BF16),
             pltpu.VMEM(value_cot.shape, BF16),
+            pltpu.VMEM(basis.shape, BF16),
+            pltpu.VMEM(master_key.shape, F32),
+            pltpu.VMEM(master_value.shape, F32),
+            pltpu.VMEM(first_key.shape, F32),
+            pltpu.VMEM(first_key.shape, F32),
+            pltpu.VMEM(first_value.shape, F32),
+            pltpu.VMEM(first_value.shape, F32),
+            pltpu.VMEM((rows, cols), BF16),
             pltpu.VMEM((tokens, rank), BF16),
             pltpu.VMEM((n, rank_rows, cols), BF16),
             pltpu.VMEM((n, rank_rows, cols), BF16),
@@ -387,21 +465,22 @@
             pltpu.VMEM((n, *small), F32),
             pltpu.VMEM(small, F32),
             pltpu.VMEM((tp, *small), F32),
-            dma((3,)),
+            dma((10,)),
         ]
         + [dma((2, 4 * lines))] * 6
         + [dma((n,))] * 4
         + [dma((tp,))] * 2,
         compiler_params=pltpu.CompilerParams(
-            collective_id=0, has_side_effects=True, vmem_limit_bytes=50 * 1024 * 1024
+            collective_id=0, has_side_effects=True, vmem_limit_bytes=67_043_328
         ),
-    )(normed, key_cot, value_cot, basis, master, first_key, second_key, first_value, second_value)
+    )(normed, key_cot, value_cot, basis, master_key, master_value, first_key, second_key, first_value, second_value)
     dirs = dirs.reshape(rank, cols)
 
-    block = 256
+    block = d // 2
     whole = lambda *shape: pl.BlockSpec(shape, lambda i: (0,) * len(shape))
     sliced = lambda width: pl.BlockSpec((block, width), lambda i: (i, 0))
-    copy_key, copy_value, step_key, step_value, new_key, new_value = pl.pallas_call(
+    moments = [whole(rank_rows, kc)] * 2 + [whole(rank_rows, vc)] * 2
+    copy_key, copy_value, step_key, step_value, new_key, new_value, nfk, nsk, nfv, nsv = pl.pallas_call(
         final_kernel,
         grid=(d // block,),
         out_shape=(
@@ -411,6 +490,10 @@
             jax.ShapeDtypeStruct((rows, vc), F32),
             jax.ShapeDtypeStruct((rows, kc), F32),
             jax.ShapeDtypeStruct((rows, vc), F32),
+            jax.ShapeDtypeStruct(first_key.shape, F32),
+            jax.ShapeDtypeStruct(first_key.shape, F32),
+            jax.ShapeDtypeStruct(first_value.shape, F32),
+            jax.ShapeDtypeStruct(first_value.shape, F32),
         ),
         in_specs=[
             sliced(rank),
@@ -419,9 +502,13 @@
             whole(rows, rank),
             whole(rows, kc),
             whole(rows, vc),
+            whole(rank_rows, cols),
+            *moments,
         ],
-        out_specs=[sliced(kc), sliced(vc), whole(rows, kc), whole(rows, vc), whole(rows, kc), whole(rows, vc)],
-    )(basis_all, master_all, dirs, basis, master_key, master_value)
+        out_specs=[sliced(kc), sliced(vc), whole(rows, kc), whole(rows, vc), whole(rows, kc), whole(rows, vc), *moments],
+    )(
+        basis_all, master_all, dirs, basis, master_key, master_value, scaled, first_key, second_key, first_value, second_value
+    )
     return (step_key, step_value, new_key, new_value, copy_key, copy_value, nfk, nsk, nfv, nsv)
 
 

time: 134 us -> 106 us (0.79)
  Pallas kernels: 121 us -> 105 us
  local copies, waits for them, and re-layouts: 9.6 us -> 0 us
  other arithmetic: 2.07 us -> 0 us
    pallas_call x1, Pallas kernels: 110 us -> 97.8 us  [on_device(): pl.pallas_call(functools.partial(exchange_kernel, n, tp, rank * cols * tp...]
    unnamed x20 -> x0, local copies, waits for them, and re-layouts: 9.6 us -> none
    pallas_call x1, Pallas kernels: 10.6 us -> 7.02 us  [on_device(): pl.pallas_call(final_kernel, grid=(d // block,), out_shape=(jax.ShapeDtyp...]
    convert_element_type x2 -> x0, other arithmetic: 2.04 us -> none  [the longest x1 1.07 us: on_device(): master_value.astype(BF16)]
where the time goes in v2:
time: 106 us; the launch traced here: 105 us
  Pallas kernels  105 us (99%)
    pallas_call x1, Pallas kernels, on_device(): pl.pallas_call(functools.partial(exchange_kernel, n, tp, rank * cols * tp...  97.8 us
    pallas_call x1, Pallas kernels, on_device(): pl.pallas_call(final_kernel, grid=(d // block,), out_shape=(jax.ShapeDtyp...  7.02 us

profile of v2, /device:TPU:0, one launch (start us, length us, event | category | flops | bytes accessed | tf_op | source)
XLA Modules:
  0.0 105.5 jit_solution(7676328255217917469)
XLA Ops:
  0.6 97.8 %shard_map.177 = (bf16[2048,256]{1,0:T(8,128)(2,1)}, bf16[2048,1536]{1,0:T(8,128)(2,1)}, bf16[16,16,1536]{2,1,0:T(8,128)(2,1)}, f32[16,1536]{1,0:T(8,128)}) custom-call(bf16[1024,2048]{1,0:T(8,128)(2,1)} %normed.1, bf16[1024,512]{1,0:T(8,128)(2,1)} %key_cot.1, bf16[1024,1024]{1,0:T(8,128)(2,1)} %value_cot.1, bf16[128,256]{1,0:T(8,128)(2,1)} %basis.1, ...), custom_call_target="tpu_custom_call" | custom-call | tf_op jit(solution)/shard_map/pallas_call | solution.py:438
  98.5 7.0 %shard_map.178 = (bf16[2048,512]{1,0:T(8,128)(2,1)}, bf16[2048,1024]{1,0:T(8,128)(2,1)}, f32[128,512]{1,0:T(8,128)}, f32[128,1024]{1,0:T(8,128)}, f32[128,512]{1...) custom-call(bf16[2048,256]{1,0:T(8,128)(2,1)} %get-tuple-element.24., ...), custom_call_target="tpu_custom_call" | custom-call | tf_op jit(solution)/shard_map/pallas_call | solution.py:483
